TPU v7x, 512 devices: a whole 4x8x8 slice. The times are simulated.
512 devices in a mesh: sp: 64 (over z, y), tp: 8 (over x, core).
Axes of the slice: x: 4, y: 8, z: 8, core: 2. Of those that a mesh axis runs over, the one named last changes fastest.
Arguments:
- resid: bfloat16 [32768, 2048], P(('sp', 'tp')), may hold values from -3 to 3
- queries: bfloat16 [32768, 1024], P('sp', 'tp'), may hold values from -6 to 6
- keys: bfloat16 [32768, 512], P('sp', 'tp'), may hold values from -6 to 6
- values: bfloat16 [32768, 512], P('sp', 'tp'), may hold values from -6 to 6
- documents: int32 [32768], P('sp'), may hold values from 0 to 31, never falling along the last dimension, each value on 1 to 2048 neighbouring positions
- sinks: float32 [16], P('tp'), may hold values from 0 to 5
- out_proj: bfloat16 [1024, 2048], replicated, may hold values from -0.75 to 0.75
- norm_gain: float32 [2048], replicated, may hold values from 0.1 to 1.9
- gate_proj: bfloat16 [2048, 5632], P('sp', 'tp'), may hold values from -0.125 to 0.125
- up_proj: bfloat16 [2048, 5632], P('sp', 'tp'), may hold values from -0.125 to 0.125
- down_proj: bfloat16 [5632, 2048], P('tp', 'sp'), may hold values from -0.078125 to 0.078125
Outputs:
- mixed: bfloat16 [32768, 2048], P(('sp', 'tp'))
Inputs may be any that keep to these rules, and one draw needn't show every extreme that they name: `documents`: document numbers never fall along the sequence; each document holds at most 2048 positions.
All inputs are finite; a program needn't handle non-finite values.
Results may differ from a plain program's by a relative error of at most 0.0095.
Values may be sent and summed in bfloat16 or wider, within the bound.
A program may use at most 64 MiB of HBM per device.

v0:
```python
import jax
import jax.numpy as jnp
from jax import lax
from jax.sharding import PartitionSpec as P

HD = 64
WINDOW = 128


def passed_along(value, axis, steps):
    count = lax.axis_size(axis)
    first, last = (max(0, -steps), min(count, count - steps))
    return lax.ppermute(value, axis, [(source, source + steps) for source in range(first, last)])


def rows_first(arrays, axis, dims):
    turned = [jnp.moveaxis(a, dim, 0) for a, dim in zip(arrays, dims)]
    widths = [t[0].size for t in turned]
    both = jnp.concatenate([t.reshape(-1, w) for t, w in zip(turned, widths)], axis=1)
    whole = lax.all_gather(both, axis, axis=0, tiled=True)
    tiles = jnp.split(whole, [sum(widths[:k]) for k in range(1, len(widths))], axis=1)
    return tuple(
        (
            jnp.moveaxis(b.reshape(-1, *t.shape[1:]), 0, dim)
            for b, t, dim in zip(tiles, turned, dims)
        )
    )


def in_order(tiles, dim):
    dims = list(tiles.shape[1:])
    dims[dim] *= tiles.shape[0]
    return jnp.moveaxis(tiles, 0, dim).reshape(dims)


def from_everyone(x, axis):
    size = lax.axis_size(axis)
    return lax.all_to_all(jnp.broadcast_to(x[None], (size, *x.shape)), axis, 0, 0, tiled=True)


def gather_directly(x, axis, dim):
    return in_order(from_everyone(x, axis), dim)


def in_blocks(x, dim, size):
    before, after = (x.shape[:dim], x.shape[dim + 1 :])
    return jnp.moveaxis(x.reshape(*before, size, -1, *after), dim, 0)


def sum_at_owner(x, axis, dim):
    size = lax.axis_size(axis)
    tiles = lax.all_to_all(in_blocks(x, dim, size), axis, 0, 0, tiled=True)
    return jnp.sum(tiles.astype(jnp.float32), axis=0)


def attend(queries, keys, values, documents, sinks):
    rows = queries.shape[0]
    kv_heads = keys.shape[1] // HD
    group = queries.shape[1] // HD // kv_heads
    blocks = rows // WINDOW
    key_value = jnp.concatenate([keys, values], axis=1)
    tail_pair, tail_docs = passed_along(
        (key_value[rows - WINDOW :], documents[rows - WINDOW :].astype(jnp.bfloat16)), "sp", 1
    )
    ext_pair = jnp.concatenate([tail_pair, key_value], axis=0).reshape(
        blocks + 1, WINDOW, 2 * kv_heads * HD
    )
    ext_docs = jnp.concatenate([tail_docs.astype(jnp.int32), documents], axis=0).reshape(
        blocks + 1, WINDOW
    )
    band = jnp.concatenate([ext_pair[:-1], ext_pair[1:]], axis=1)
    band_keys = band[:, :, : kv_heads * HD].reshape(blocks, 2 * WINDOW, kv_heads, HD)
    band_values = band[:, :, kv_heads * HD :].reshape(blocks, 2 * WINDOW, kv_heads, HD)
    band_docs = jnp.concatenate([ext_docs[:-1], ext_docs[1:]], axis=1)
    query_docs = documents.reshape(blocks, WINDOW)
    offset = lax.axis_index("sp") * rows
    distance = jnp.arange(WINDOW)[:, None] + WINDOW - jnp.arange(2 * WINDOW)[None, :]
    key_pos = (
        offset + jnp.arange(blocks)[:, None] * WINDOW + jnp.arange(2 * WINDOW)[None, :] - WINDOW
    )
    visible = (
        ((distance >= 0) & (distance < WINDOW))[None]
        & (key_pos >= 0)[:, None, :]
        & (band_docs[:, None, :] == query_docs[:, :, None])
    )
    query_blocks = queries.reshape(blocks, WINDOW, kv_heads, group, HD)
    scores = jnp.einsum(
        "nikgd,njkd->nkgij", query_blocks, band_keys, preferred_element_type=jnp.float32
    ) * HD ** (-0.5)
    scores = jnp.where(visible[:, None, None], scores, -jnp.inf)
    sink_logit = sinks.reshape(kv_heads, group)[None, :, :, None, None]
    row_top = jnp.maximum(jnp.max(scores, axis=-1, keepdims=True), sink_logit)
    raw_weights = jnp.exp(scores - row_top)
    totals = jnp.sum(raw_weights, axis=-1, keepdims=True) + jnp.exp(sink_logit - row_top)
    weights = (raw_weights / totals).astype(jnp.bfloat16)
    attended = jnp.einsum(
        "nkgij,njkd->nikgd", weights, band_values, preferred_element_type=jnp.float32
    )
    return attended.astype(jnp.bfloat16).reshape(rows, kv_heads * group * HD)


def norm_rows(mid_rows, norm_gain):
    scale = lax.rsqrt(jnp.mean(mid_rows * mid_rows, axis=-1, keepdims=True) + 1e-06)
    return (mid_rows * scale * norm_gain).astype(jnp.bfloat16)


def shards(
    resid,
    queries,
    keys,
    values,
    documents,
    sinks,
    out_proj,
    norm_gain,
    gate_proj,
    up_proj,
    down_proj,
):
    gate_whole, up_whole, down_whole = rows_first((gate_proj, up_proj, down_proj), "sp", (0, 0, 1))
    attended = attend(queries, keys, values, documents, sinks)
    own_heads = lax.all_to_all(attended, "tp", split_axis=0, concat_axis=1, tiled=True)
    mid_rows = resid.astype(jnp.float32) + jnp.dot(
        own_heads, out_proj, preferred_element_type=jnp.float32
    )
    normed = gather_directly(norm_rows(mid_rows, norm_gain), "tp", 0)
    gate_acts = jnp.dot(normed, gate_whole, preferred_element_type=jnp.float32)
    up_acts = jnp.dot(normed, up_whole, preferred_element_type=jnp.float32)
    hidden = (jax.nn.silu(gate_acts) * up_acts).astype(jnp.bfloat16)
    summed = sum_at_owner(
        jnp.dot(hidden, down_whole, preferred_element_type=jnp.float32).astype(jnp.bfloat16),
        "tp",
        0,
    )
    return (mid_rows + summed).astype(jnp.bfloat16)


def solution(mesh):
    in_specs = (
        P(("sp", "tp"), None),
        P("sp", "tp"),
        P("sp", "tp"),
        P("sp", "tp"),
        P("sp"),
        P("tp"),
        P(),
        P(),
        P("sp", "tp"),
        P("sp", "tp"),
        P("tp", "sp"),
    )
    out_specs = P(("sp", "tp"), None)
    return jax.shard_map(shards, mesh=mesh, in_specs=in_specs, out_specs=out_specs, check_vma=False)
```

profile of v0, /device:TPU:1, one launch (start us, length us, event | category | flops | bytes accessed | tf_op | source)
XLA Modules:
  0.0 170.7 jit_solution(16067916554664489220)
XLA Ops:
  6.5 0.0 all-gather.2.cloned.1.call-start
  6.5 1.6 concatenate.23
  8.1 0.0 all-gather.2.cloned.1.call-update
  8.2 0.0 copy-start.2
  8.2 0.7 convert.3
  8.9 4.0 %collective-permute-start.1 = (bf16[128]{0:T(256)(128)(2,1)S(1)}, bf16[128]{0:T(256)(128)(2,1)S(1)}, u32[]{:S(2)}, u32[]{:S(2)}) collective-permute-start(bf16[128]{0:T(256)(128)(2,1)S(1)} %slice.48), channel_id=1, source_target_pairs={{0,8},{8,16},{16,24},{24,32},{32,40},{40,48},{48,56},{56,64},{64,7... | collective-permute-start | bytes 776 | tf_op jit(solution)/shard_map/ppermute | solution.py:13
  12.9 1.0 copy.23
  13.9 1.0 copy.24
  14.8 0.1 fusion.35
  14.9 3.2 %collective-permute-start = (bf16[128,128]{1,0:T(8,128)(2,1)S(1)}, bf16[128,128]{1,0:T(8,128)(2,1)S(1)}, u32[]{:S(2)}, u32[]{:S(2)}) collective-permute-start(bf16[128,128]{1,0:T(8,128)(2,1)S(1)} %fusion.35), channel_id=1, source_target_pairs={{0,8},{8,16},{16,24},{24,32},{32,40},{40,48},{48,56},{56,64},{64,7... | collective-permute-start | bytes 98312 | tf_op jit(solution)/shard_map/ppermute | solution.py:13
  18.2 0.1 add_compare_fusion
  18.3 1.0 reshape.150
  19.3 0.0 collective-permute-done.1
  19.4 0.7 pad_add_fusion
  20.1 0.7 pad_add_fusion.1
  20.7 1.0 compare_and_fusion
  21.8 0.0 collective-permute-done
  21.8 0.1 pad_maximum_fusion.1
  21.9 0.1 copy.25
  22.1 0.1 copy.26
  22.2 0.4 fusion.39
  22.6 0.0 copy-done.2
  22.6 0.1 broadcast_maximum_fusion
  22.6 0.2 fusion.20
  22.8 0.1 exponential_add_fusion
  22.9 0.0 copy-start
  22.9 0.3 fusion.19
  23.2 0.2 copy.38
  23.4 0.1 reshape.151
  23.5 10.6 %all_to_all.29 = bf16[8,64,128]{2,1,0:T(8,128)(2,1)S(1)} all-to-all(bf16[8,64,128]{2,1,0:T(8,128)(2,1)S(1)} %reshape.151), channel_id=1, replica_groups=mesh['sp'=64,'tp'=8] {'tp'}, dimensions={0} | all-to-all | bytes 262144 | tf_op jit(solution)/shard_map/all_to_all | solution.py:122
  34.1 0.0 copy-done
  34.1 0.0 copy-start.1
  34.1 3.2 %multiply_reduce_fusion = (f32[64]{0:T(128)S(1)}, f32[64,2048]{1,0:T(8,128)S(1)}) fusion(bf16[1024,2048]{1,0:T(8,128)(2,1)} %param.17, bf16[64,2048]{1,0:T(8,128)(2,1)S(1)} %copy-done, bf16[8,64,128]{2,1,0:T(8,128)(2,1)S(1)} %all_to_all.29), kind=kOutput, calls=%fused_computation.23 | convolution fusion | flops 268959680 | bytes 5112064 | tf_op jit(solution)/shard_map/dot_general | solution.py:123
  37.3 0.0 copy-done.1
  37.3 0.1 multiply_convert_fusion
  37.5 0.2 broadcast_in_dim.16
  37.7 29.5 %all_to_all.30 = bf16[8,64,2048]{2,1,0:T(8,128)(2,1)S(1)} all-to-all(bf16[8,64,2048]{2,1,0:T(8,128)(2,1)S(1)} %broadcast_in_dim.16), channel_id=1, replica_groups=mesh['sp'=64,'tp'=8] {'tp'}, dimensions={0} | all-to-all | bytes 4194304 | tf_op jit(solution)/shard_map/all_to_all | solution.py:38
  67.2 50.1 %all-gather.2.cloned.1.call-done = bf16[2048,2112]{1,0:T(8,128)(2,1)} async-done(((bf16[32,2112]{1,0:T(8,128)(2,1)}), bf16[2048,2112]{1,0:T(8,128)(2,1)}) %all-gather.2.cloned.1.call-update) | async-done | bytes 8650768 | tf_op jit(solution)/shard_map/all_gather | solution.py:20
  117.3 4.7 %fusion.4 = f32[512,704]{0,1:T(8,128)} fusion(bf16[512,2048]{1,0:T(8,128)(2,1)S(1)} %bitcast.48, bf16[2048,2112]{1,0:T(8,128)(2,1)} %all-gather.2.cloned.1.call-done), kind=kOutput, calls=%fused_computation.5 | convolution fusion | flops 1476395008 | bytes 6684672 | tf_op jit(solution)/shard_map/dot_general | solution.py:127
  121.9 9.5 %fusion.6 = bf16[512,2048]{1,0:T(8,128)(2,1)} fusion(bf16[2048,2112]{1,0:T(8,128)(2,1)} %all-gather.2.cloned.1.call-done, bf16[512,2048]{1,0:T(8,128)(2,1)S(1)} %bitcast.49, f32[512,704]{0,1:T(8,128)} %fusion.4), kind=kOutput, calls=%fused_computation.7 | convolution fusion | flops 2956001280 | bytes 11927552 | tf_op jit(solution)/shard_map/dot_general | solution.py:131
  131.4 31.3 %all_to_all.31 = bf16[8,64,2048]{2,1,0:T(8,128)(2,1)S(1)} all-to-all(bf16[8,64,2048]{2,1,0:T(8,128)(2,1)} %bitcast.50), channel_id=1, replica_groups=mesh['sp'=64,'tp'=8] {'tp'}, dimensions={0} | all-to-all | bytes 4194304 | tf_op jit(solution)/shard_map/all_to_all | solution.py:52
  162.7 0.4 convert_reduce_fusion
  163.1 0.8 add_convert_fusion
  (7 shorter events, 0.1 us)
Async XLA Ops:
  6.5 110.7 %all-gather.2.cloned.1.call-start = ((), (), s32[]{:S(2)}) async-start(), calls=%async_computation.3 | async-start | bytes 9052160 | tf_op jit(solution)/shard_map/all_gather | solution.py:20
  8.2 14.4 %copy-start.2 = (f32[2]{0:T(128)S(1)}, f32[2]{0:T(128)}, u32[]{:S(2)}) copy-start(f32[2]{0:T(128)} %param.16) | copy-start | bytes 28
  8.9 10.5 %collective-permute-start.1 = (bf16[128]{0:T(256)(128)(2,1)S(1)}, bf16[128]{0:T(256)(128)(2,1)S(1)}, u32[]{:S(2)}, u32[]{:S(2)}) collective-permute-start(bf16[128]{0:T(256)(128)(2,1)S(1)} %slice.48), channel_id=1, source_target_pairs={{0,8},{8,16},{16,24},{24,32},{32,40},{40,48},{48,56},{56,64},{64,7... | collective-permute-start | bytes 776 | tf_op jit(solution)/shard_map/ppermute | solution.py:13
  14.9 6.8 %collective-permute-start = (bf16[128,128]{1,0:T(8,128)(2,1)S(1)}, bf16[128,128]{1,0:T(8,128)(2,1)S(1)}, u32[]{:S(2)}, u32[]{:S(2)}) collective-permute-start(bf16[128,128]{1,0:T(8,128)(2,1)S(1)} %fusion.35), channel_id=1, source_target_pairs={{0,8},{8,16},{16,24},{24,32},{32,40},{40,48},{48,56},{56,64},{64,7... | collective-permute-start | bytes 98312 | tf_op jit(solution)/shard_map/ppermute | solution.py:13
  22.9 11.2 %copy-start = (bf16[64,2048]{1,0:T(8,128)(2,1)S(1)}, bf16[64,2048]{1,0:T(8,128)(2,1)}, u32[]{:S(2)}) copy-start(bf16[64,2048]{1,0:T(8,128)(2,1)} %param.11) | copy-start | bytes 786436
  34.1 3.2 %copy-start.1 = (f32[2048]{0:T(1024)S(1)}, f32[2048]{0:T(1024)}, u32[]{:S(2)}) copy-start(f32[2048]{0:T(1024)} %param.18) | copy-start | bytes 24580
Sparse Core Ops, SparseCore 0:
  10.3 106.8 all-gather.1
where the time goes:
time: 171 us
  blocking collectives  71.3 us (42%)
  waiting for transfers between devices  50.1 us (29%)
  matrix products  18 us (11%)
  between operations  13.6 us (8%)
  starting transfers between devices  7.21 us (4%)
  local copies, waits for them, and re-layouts  5.42 us (3%)
  other arithmetic  5 us (3%)
    all_gather x1, waiting for transfers between devices, rows_first(): whole = lax.all_gather(both, axis, axis=0, tiled=True)  50.1 us
    all_to_all x1, blocking collectives, sum_at_owner(): tiles = lax.all_to_all(in_blocks(x, dim, size), axis, 0, 0, tiled=True)  31.3 us
    all_to_all x1, blocking collectives, from_everyone(): lax.all_to_all(jnp.broadcast_to(x[None], (size, *x.shape)), axis, 0, 0, t...  29.5 us
    all_to_all x1, blocking collectives, shards(): lax.all_to_all(attended, 'tp', split_axis=0, concat_axis=1, tiled=True)  10.6 us
    dot_general x1, matrix products, shards(): jnp.dot(hidden, down_whole, preferred_element_type=jnp.float32)  9.48 us
    ppermute x2, starting transfers between devices, passed_along(): lax.ppermute(value, axis, [(source, source + steps) for source in range(f...  7.21 us
    dot_general x1, matrix products, shards(): gate_acts = jnp.dot(normed, gate_whole, preferred_element_type=jnp.float32)  4.67 us
  transfers between devices with their start and end apart: 3, of which 1 were waited for; matrix products, arithmetic and copies ran while one was open for 7% of the time, Pallas kernels for 0%

commit v1 on v0

v1 whole, which is shorter than its diff:
```python
import jax
import jax.numpy as jnp
from jax import lax
from jax.experimental import pallas as pl
from jax.experimental.pallas import tpu as pltpu
from jax.sharding import PartitionSpec as P

MESH = pl.DeviceIdType.MESH
F32, BF16 = jnp.float32, jnp.bfloat16
SIDE = 8
REL = (0, -1, 1, -2, 2, -3, 3, -4)
LAST = {1: 4, -1: 3}
BOTH = (1, -1)
SEMS = 160


def wrap(value, offset):
    return lax.rem(value + (offset + SIDE), SIDE) if offset else value


def unit_of(stage, half, sign):
    if stage == 0:
        return half
    if stage == 4:
        return 14 + half
    return 4 * stage - 2 + 2 * half + (0 if sign > 0 else 1)


def dot(a, b):
    return jnp.dot(a, b, preferred_element_type=F32)


def dot_t(a, b):
    return lax.dot_general(a, b, (((1,), (1,)), ((), ())), preferred_element_type=F32)


def layer(
    sinks, resid, q, kt, vt, docs, gain, gu, dn, op_hbm, out,
    wg, wd, op, nb, at, ka, kb, va, vb, hk, hv, dh, ed, att, mid, hid,
    pb, pr, qb, rx, ss, tn, tt, send, recv, local,
):
    sp, tp = lax.axis_index("sp"), lax.axis_index("tp")
    y, z = lax.rem(sp, SIDE), lax.div(sp, SIDE)
    x, core = lax.rem(lax.div(tp, 2), 4), lax.rem(tp, 2)
    other = 1 - core
    partner = (sp, 2 * x + other)
    ahead = lax.rem(sp + 1, SIDE * SIDE)
    behind = lax.rem(sp + SIDE * SIDE - 1, SIDE * SIDE)

    def place(dy, dz):
        return (wrap(z, dz) * SIDE + wrap(y, dy), tp)

    def toward(half, ring, sign):
        return place(sign, 0) if half == ring else place(0, sign)

    def chip(j):
        return lax.rem(x + j, 4)

    barrier = pltpu.get_barrier_semaphore()
    greeted = [place(1, 0), place(-1, 0), place(0, 1), place(0, -1)]
    greeted += [(ahead, tp), (behind, tp)]
    greeted += [(sp, lax.rem(tp + j, 8)) for j in range(1, 8)]
    for where in greeted:
        pl.semaphore_signal(barrier, inc=1, device_id=where, device_id_type=MESH)

    own_op = pltpu.make_async_copy(op_hbm, op, local.at[0])
    own_gu = pltpu.make_async_copy(gu, wg.at[z, y], local.at[1])
    own_dn = [
        pltpu.make_async_copy(dn.at[pl.ds(16 * h, 16)], wd.at[h, 0], local.at[2 + h]) for h in (0, 1)
    ]
    for copy in (own_gu, *own_dn, own_op):
        copy.start()

    pl.semaphore_wait(barrier, len(greeted))

    pending = []

    def go(src, dst, where):
        n = len(pending)
        copy = pltpu.make_async_remote_copy(
            src_ref=src, dst_ref=dst, send_sem=send.at[n], recv_sem=recv.at[n],
            device_id=where, device_id_type=MESH,
        )
        copy.start()
        pending.append(copy)
        return copy

    def gu_at(half, near):
        rows = pl.ds(16 * half, 16)
        return wg.at[z, wrap(y, near), rows] if half == 0 else wg.at[wrap(z, near), y, rows]

    def gu_own(half):
        return gu.at[pl.ds(16 * half, 16)]

    def gu_part(half, far, part):
        rows, some = pl.ds(16 * half, 16), pl.ds(4 * part, 4)
        return wg.at[wrap(z, far), some, rows] if half == 0 else wg.at[some, wrap(y, far), rows]

    near_gu, far_gu, near_dn, far_dn = {}, {}, {}, {}

    def inject(half, near, src=None):
        block = gu_at(half, near)
        for sign in BOTH:
            far_gu[half, sign, near] = go(block if src is None else src, block, toward(half, 1, sign))

    def gu_step(k):
        for half in (0, 1):
            for sign in BOTH:
                if k > LAST[sign]:
                    continue
                near_gu[half, sign, k].wait_recv()
                block = gu_at(half, -sign * k)
                if k < LAST[sign]:
                    near_gu[half, sign, k + 1] = go(block, block, toward(half, 0, sign))
                inject(half, -sign * k)

    def gu_send(stage, half, sign, part):
        block = gu_part(half, -sign * (stage - 1), part)
        far_gu[stage, half, sign, part] = go(block, block, toward(half, 1, sign))

    def dn_first(half, sign, k, src=None):
        src = wd.at[half, REL.index(-sign * (k - 1))] if src is None else src
        near_dn[half, sign, k] = go(src, wd.at[half, REL.index(-sign * k)], toward(half, 0, sign))

    def dn_step(k):
        for half in (0, 1):
            for sign in BOTH:
                if k <= LAST[sign]:
                    near_dn[half, sign, k].wait_recv()
                    if k < LAST[sign]:
                        dn_first(half, sign, k + 1)

    def dn_send(stage, half, sign, part):
        some = pl.ds(4 * part, 4)
        far_dn[stage, half, sign, part] = go(
            wd.at[unit_of(stage - 1, half, sign), some],
            wd.at[unit_of(stage, half, sign), some],
            toward(half, 1, sign),
        )

    def dn_pass(stage, part):
        for half in (0, 1):
            for sign in BOTH:
                far_dn[stage, half, sign, part].wait_recv()
                if stage < 3 or part == (0 if sign > 0 else 1):
                    dn_send(stage + 1, half, sign, part)

    for half in (0, 1):
        for sign in BOTH:
            near_gu[half, sign, 1] = go(gu_own(half), gu_at(half, 0), toward(half, 0, sign))
    for half in (0, 1):
        inject(half, 0, gu_own(half))
    tail = pl.ds(384, 128)
    halo = [
        go(kt.at[:, tail], hk, (ahead, tp)),
        go(vt.at[:, tail], hv, (ahead, tp)),
        go(docs, dh, (ahead, tp)),
    ]

    for first, second, source in ((ka, kb, kt), (va, vb, vt)):
        first[64:128, :] = jnp.zeros((64, 640), BF16)
        second[0:64, :] = jnp.zeros((64, 640), BF16)
        first[0:64, 128:640] = source[...]
        second[64:128, 128:640] = source[...]
    for block in range(4):
        ed[0:1, 128 * (block + 1) : 128 * (block + 2)] = docs[block : block + 1, :].astype(F32)

    def attend(block):
        rows, span = pl.ds(128 * block, 128), pl.ds(128 * block, 256)
        query_docs = jnp.broadcast_to(ed[0:1, 128 * (block + 1) : 128 * (block + 2)], (128, 128)).T
        query_docs = jnp.concatenate([query_docs, query_docs], axis=1)
        at_query = lax.broadcasted_iota(jnp.int32, (128, 256), 0)
        at_key = lax.broadcasted_iota(jnp.int32, (128, 256), 1)
        visible = (at_key > at_query) & (at_key <= at_query + 128)
        visible = visible & (ed[0:1, 128 * block : 128 * block + 256] == query_docs)
        total = None
        for head, keys, vals in ((0, ka, va), (1, kb, vb)):
            scores = dot(q[rows, :], keys[:, span]) * 0.125
            scores = jnp.where(visible, scores, -jnp.inf)
            sink = sinks[head]
            top = jnp.maximum(jnp.max(scores, axis=1, keepdims=True), sink)
            raw = jnp.exp(scores - top)
            whole = jnp.sum(raw, axis=1, keepdims=True) + jnp.exp(sink - top)
            weights = (raw / whole).astype(BF16)
            part = dot_t(weights, vals[:, span])
            total = part if total is None else total + part
        att[rows, :] = total.astype(BF16)

    for block in (1, 2, 3):
        attend(block)
    gu_step(1)
    for copy in halo:
        copy.wait_recv()
    ka[0:64, 0:128] = hk[...]
    kb[64:128, 0:128] = hk[...]
    va[0:64, 0:128] = hv[...]
    vb[64:128, 0:128] = hv[...]
    ed[0:1, 0:128] = jnp.where(sp == 0, -1.0, dh[3:4, :].astype(F32))
    attend(0)
    lanes = pl.ds(pl.multiple_of(128 * tp, 128), 128)
    heads = []
    for j in range(1, 8):
        peer = lax.rem(tp + j, 8)
        rows = pl.ds(pl.multiple_of(64 * peer, 64), 64)
        heads.append(go(att.at[rows], at.at[:, lanes], (sp, peer)))
    own_rows = pl.ds(pl.multiple_of(64 * tp, 64), 64)
    at[:, lanes] = att[own_rows, :]
    gu_step(2)

    for copy in heads:
        copy.wait_recv()
    own_op.wait()
    for part in range(8):
        cols = pl.ds(256 * part, 256)
        mid[:, cols] = resid[:, cols].astype(F32) + dot(at[...], op[:, cols])
    rows64 = mid[...]
    scale = lax.rsqrt(jnp.mean(rows64 * rows64, axis=1, keepdims=True) + 1e-06)
    nb[own_rows, :] = (rows64 * scale * gain[...]).astype(BF16)
    rows_out = {}
    for j in (0, 1, 3, 2):
        where = partner if j == 0 else (sp, 2 * chip(j) + core)
        rows_out[j] = go(nb.at[own_rows], nb.at[own_rows], where)
    gu_step(3)
    gu_step(4)
    for half in (0, 1):
        for sign in BOTH:
            dn_first(half, sign, 1, dn.at[pl.ds(16 * half, 16)])
    for half in (0, 1):
        for sign in BOTH:
            for near in REL:
                far_gu[half, sign, near].wait_recv()
            for part in (0, 1):
                gu_send(2, half, sign, part)
    dn_step(1)

    def gu_pass(stage, part):
        for half in (0, 1):
            for sign in BOTH:
                far_gu[stage, half, sign, part].wait_recv()
                if stage < 3 or part == (0 if sign > 0 else 1):
                    gu_send(stage + 1, half, sign, part)

    passed = []

    def rows_on(j):
        rows_out[j].wait_recv()
        rows = pl.ds(pl.multiple_of(64 * (2 * chip(4 - j) + core), 64), 64)
        passed.append(go(nb.at[rows], nb.at[rows], partner))

    gu_pass(2, 0)
    rows_on(1)
    rows_on(3)
    gu_pass(2, 1)
    rows_on(2)
    dn_step(2)
    gu_pass(3, 0)
    gu_pass(3, 1)
    for copy in own_dn:
        copy.wait()
    for half in (0, 1):
        for sign in BOTH:
            dn_send(1, half, sign, 0)
    dn_step(3)
    dn_step(4)
    for half in (0, 1):
        for sign in BOTH:
            dn_send(1, half, sign, 1)
    rows_out[0].wait_recv()
    for copy in passed:
        copy.wait_recv()
    own_gu.wait()
    for half in (0, 1):
        for sign in BOTH:
            far_gu[4, half, sign, 0 if sign > 0 else 1].wait_recv()

    def columns(first, width):
        return wg[:, :, :, first : first + width].reshape(SIDE * SIDE * 32, width)

    def silu(v):
        return v / (1.0 + jnp.exp(-v))

    def hidden_part(i):
        gate = dot(nb[...], columns(256 * i, 256))
        if i < 2:
            up = dot(nb[...], columns(768 + 256 * i, 256))
            hid[:, 256 * i : 256 * (i + 1)] = (silu(gate) * up).astype(BF16)
            return
        up = dot(nb[...], columns(1280, 128))
        hid[:, 512:640] = (silu(gate[:, :128]) * up).astype(BF16)
        mixed = gate[:, 128:]
        lane = lax.broadcasted_iota(jnp.int32, mixed.shape, 1)
        ends = silu(mixed) * pltpu.roll(mixed, 64, 1)
        hid[:, 640:768] = jnp.where(lane < 64, ends, 0.0).astype(BF16)

    summed = {}

    def partial_of(stage):
        first = unit_of(stage, 0, 1)
        count = 2 if stage in (0, 4) else 4
        size, base = 64 * count, 128 * first
        units = wd[first : first + count].reshape(128 * count, 768)
        pb[base : base + 2 * size, :] = dot_t(units, hid[...]).astype(BF16)
        theirs = pl.ds(pl.multiple_of(base + size * other, 128), size)
        summed[stage] = go(pb.at[theirs], pr.at[pl.ds(64 * first, size)], partner)

    sums = []

    def chip_sum(stage):
        first = unit_of(stage, 0, 1)
        size = 128 if stage in (0, 4) else 256
        summed[stage].wait_recv()
        ours = pl.ds(pl.multiple_of(128 * first + size * core, 128), size)
        rows = pl.ds(64 * first, size)
        qb[rows, :] = (pb[ours, :].astype(F32) + pr[rows, :].astype(F32)).astype(BF16)
        for j in (2, 1, 3):
            tokens = pl.ds(pl.multiple_of(128 * chip(j), 128), 128)
            sums.append(go(qb.at[rows, tokens], rx.at[j - 1, rows], (sp, 2 * chip(j) + core)))

    hidden_part(0)
    hidden_part(1)
    dn_pass(1, 0)
    hidden_part(2)
    partial_of(0)
    dn_pass(1, 1)
    partial_of(1)
    chip_sum(0)
    chip_sum(1)
    dn_pass(2, 0)
    dn_pass(2, 1)
    partial_of(2)
    chip_sum(2)
    dn_pass(3, 0)
    dn_pass(3, 1)
    partial_of(3)
    chip_sum(3)
    for half in (0, 1):
        for sign in BOTH:
            far_dn[4, half, sign, 0 if sign > 0 else 1].wait_recv()
    partial_of(4)
    chip_sum(4)
    for copy in sums:
        copy.wait_recv()
    tokens = pl.ds(pl.multiple_of(128 * x, 128), 128)
    mine = qb[:, tokens].astype(F32)
    for j in range(3):
        mine = mine + rx[j].astype(F32)
    ss[core] = mine.astype(BF16)
    last = go(ss.at[core], ss.at[core], partner)
    last.wait_recv()
    fars = (0, -1, 1, -2, 2, -3, 3, -4)
    for half in (0, 1):
        for i, far in enumerate(fars):
            for r, near in enumerate(REL):
                dy, dz = (near, far) if half == 0 else (far, near)
                row = 256 * wrap(z, dz) + 32 * wrap(y, dy) + 16 * half
                first = 128 * i + 16 * r
                tn[pl.ds(pl.multiple_of(row, 16), 16), :] = ss[half, first : first + 16, :].astype(F32)
    for part in range(16):
        tt[:, 128 * part : 128 * (part + 1)] = tn[128 * part : 128 * (part + 1), :].T
    out[...] = (mid[...] + tt[pl.ds(pl.multiple_of(64 * core, 64), 64), :]).astype(BF16)
    for copy in pending:
        copy.wait_send()


def shards(
    resid, queries, keys, values, documents, sinks, out_proj, norm_gain, gate_proj, up_proj, down_proj
):
    gu = jnp.concatenate([gate_proj, up_proj[:, 640:], up_proj[:, :640]], axis=1)
    dn = jnp.pad(down_proj.T, ((0, 0), (0, 64)))
    vmem = pl.BlockSpec(memory_space=pltpu.VMEM)
    return pl.pallas_call(
        layer,
        out_shape=jax.ShapeDtypeStruct((64, 2048), BF16),
        in_specs=[pl.BlockSpec(memory_space=pltpu.SMEM)]
        + [vmem] * 8
        + [pl.BlockSpec(memory_space=pl.ANY)],
        out_specs=vmem,
        scratch_shapes=[
            pltpu.VMEM((8, 8, 32, 1408), BF16),
            pltpu.VMEM((16, 8, 16, 768), BF16),
            pltpu.VMEM((1024, 2048), BF16),
            pltpu.VMEM((512, 2048), BF16),
            pltpu.VMEM((64, 1024), BF16),
            pltpu.VMEM((128, 640), BF16),
            pltpu.VMEM((128, 640), BF16),
            pltpu.VMEM((128, 640), BF16),
            pltpu.VMEM((128, 640), BF16),
            pltpu.VMEM((64, 128), BF16),
            pltpu.VMEM((64, 128), BF16),
            pltpu.VMEM((4, 128), jnp.int32),
            pltpu.VMEM((8, 640), F32),
            pltpu.VMEM((512, 128), BF16),
            pltpu.VMEM((64, 2048), F32),
            pltpu.VMEM((512, 768), BF16),
            pltpu.VMEM((2048, 512), BF16),
            pltpu.VMEM((1024, 512), BF16),
            pltpu.VMEM((1024, 512), BF16),
            pltpu.VMEM((3, 1024, 128), BF16),
            pltpu.VMEM((2, 1024, 128), BF16),
            pltpu.VMEM((2048, 128), F32),
            pltpu.VMEM((128, 2048), F32),
            pltpu.SemaphoreType.DMA((SEMS,)),
            pltpu.SemaphoreType.DMA((SEMS,)),
            pltpu.SemaphoreType.DMA((4,)),
        ],
        compiler_params=pltpu.CompilerParams(
            collective_id=0, has_side_effects=True, vmem_limit_bytes=60 * 1024 * 1024
        ),
        name="layer",
    )(
        sinks, resid, queries, keys.T, values.T, documents.reshape(4, 128),
        norm_gain.reshape(1, 2048), gu, dn, out_proj,
    )


def solution(mesh):
    in_specs = (
        P(("sp", "tp"), None),
        P("sp", "tp"),
        P("sp", "tp"),
        P("sp", "tp"),
        P("sp"),
        P("tp"),
        P(),
        P(),
        P("sp", "tp"),
        P("sp", "tp"),
        P("tp", "sp"),
    )
    out_specs = P(("sp", "tp"), None)
    return jax.shard_map(shards, mesh=mesh, in_specs=in_specs, out_specs=out_specs, check_vma=False)
```

time: 171 us -> 94.8 us (0.55)
  Pallas kernels: 0 us -> 88.3 us
  blocking collectives: 71.3 us -> 0 us
  waiting for transfers between devices: 50.1 us -> 0 us
  matrix products: 18 us -> 0 us
  between operations: 13.6 us -> 0.01 us
  starting transfers between devices: 7.21 us -> 0 us
  other arithmetic: 5 us -> 0 us
    pallas_call x0 -> x1, Pallas kernels: none -> 88.3 us  [shards(): pl.pallas_call(layer, out_shape=jax.ShapeDtypeStruct((64, 2048), BF16), i...]
    all_to_all x3 -> x0, blocking collectives: 71.3 us -> none  [the longest x1 31.3 us: sum_at_owner(): tiles = lax.all_to_all(in_blocks(x, dim, size), axis, 0, 0, tiled=True)]
    all_gather x1 -> x0, waiting for transfers between devices: 50.1 us -> none  [rows_first(): whole = lax.all_gather(both, axis, axis=0, tiled=True)]
    dot_general x5 -> x0, matrix products: 18 us -> none  [the longest x1 9.48 us: shards(): jnp.dot(hidden, down_whole, preferred_element_type=jnp.float32)]
    ppermute x2 -> x0, starting transfers between devices: 7.21 us -> none  [passed_along(): lax.ppermute(value, axis, [(source, source + steps) for source in range(f...]
  transfers between devices with their start and end apart: 3 -> 0, of which waited for: 1 -> 0; matrix products, arithmetic and copies ran while one was open for 7% -> 0% of each run, Pallas kernels for 0% -> 0%
where the time goes in v1:
time: 94.8 us; the launch traced here: 94.4 us
  Pallas kernels  88.3 us (93%)
  local copies, waits for them, and re-layouts  6.09 us (6%)
    pallas_call x1, Pallas kernels, shards(): pl.pallas_call(layer, out_shape=jax.ShapeDtypeStruct((64, 2048), BF16), i...  88.3 us

profile of v1, /device:TPU:1, one launch (start us, length us, event | category | flops | bytes accessed | tf_op | source)
XLA Modules:
  0.0 94.4 jit_solution(5561018404291964881)
XLA Ops:
  0.0 0.7 slice.6
  0.7 0.8 slice.7
  1.5 1.5 %concatenate.3.gu = bf16[32,1408]{1,0:T(8,128)(2,1)} concatenate(bf16[32,704]{1,0:T(8,128)(2,1)} %param.19, bf16[32,64]{1,0:T(8,128)(2,1)S(1)} %slice.6, bf16[32,640]{1,0:T(8,128)(2,1)S(1)} %slice.7), dimensions={1} | concatenate | bytes 180224 | tf_op jit(solution)/shard_map/concatenate | solution.py:368
  3.0 1.4 %pad.4.dn = bf16[32,768]{1,0:T(8,128)(2,1)} pad(bf16[32,704]{1,0:T(8,128)(2,1)} %bitcast.7, bf16[]{:T(256)} %constant.2.clone.1), padding=0_0x0_64 | pad | bytes 94210 | tf_op jit(solution)/shard_map/jit(_pad)/pad | solution.py:369
  4.4 88.3 %layer.1 = bf16[64,2048]{1,0:T(8,128)(2,1)} custom-call(f32[2]{0:T(128)} %sinks.1, bf16[64,2048]{1,0:T(8,128)(2,1)} %resid.1, bf16[512,128]{1,0:T(8,128)(2,1)} %q.1, bf16[64,512]{1,0:T(8,128)(2,1)} %bitcast.5, bf16[64,512]{1,0:T(8,128)(2,1)} %bitcast.6, s32[4,128]{1,0:T(4,128)} %bitcast.9, f32[1,2048]{1,0:T(1,128)} %bitcast.8, ...), custom_call_target="tpu_custom_call" | custom-call | tf_op jit(solution)/shard_map/layer/pallas_call | solution.py:371
  92.7 1.7 %copy.13 = bf16[64,2048]{1,0:T(8,128)(2,1)} copy(bf16[64,2048]{1,0:T(8,128)(2,1)} %layer.1) | data formatting | bytes 524288

commit v2 on v1

v2 whole, which is shorter than its diff:
```python
import math

import jax
import jax.numpy as jnp
from jax import lax
from jax.experimental import pallas as pl
from jax.experimental.pallas import tpu as pltpu
from jax.sharding import PartitionSpec as P

MESH = pl.DeviceIdType.MESH
F32, BF16 = jnp.float32, jnp.bfloat16
SIDE = 8
REL = (0, -1, 1, -2, 2, -3, 3, -4)
LAST = {1: 4, -1: 3}
BOTH = (1, -1)
SEMS = 64
NEARS = ((0,), (-1, 1), (-2, 2), (-3, 3), (-4,))


def wrap(value, offset):
    return lax.rem(value + (offset + SIDE), SIDE) if offset else value


def unit_of(stage, half, sign):
    if stage == 0:
        return half
    if stage == 4:
        return 14 + half
    return 4 * stage - 2 + 2 * half + (0 if sign > 0 else 1)


def dot(a, b):
    return jnp.dot(a, b, preferred_element_type=F32)


def dot_t(a, b):
    return lax.dot_general(a, b, (((1,), (1,)), ((), ())), preferred_element_type=F32)


def layer(
    sinks, resid_hbm, q_hbm, kt_hbm, vt_hbm, docs_hbm, gain_hbm, gate_hbm, up_hbm, dt_hbm, op_hbm, out,
    resid, q, kt, vt, docs, gain, gate_own, up_own, dt_own, wg, wd, op, nb, at, ka, kb, va, vb, hk, hv, dh, ed, att, mid, hid,
    pb, pr, qb, rx, ss, tn, tt, send, recv, local,
):
    sp, tp = lax.axis_index("sp"), lax.axis_index("tp")
    y, z = lax.rem(sp, SIDE), lax.div(sp, SIDE)
    x, core = lax.rem(lax.div(tp, 2), 4), lax.rem(tp, 2)
    other = 1 - core
    partner = (sp, 2 * x + other)
    ahead = lax.rem(sp + 1, SIDE * SIDE)
    behind = lax.rem(sp + SIDE * SIDE - 1, SIDE * SIDE)

    def place(dy, dz):
        return (wrap(z, dz) * SIDE + wrap(y, dy), tp)

    def toward(half, ring, sign):
        return place(sign, 0) if half == ring else place(0, sign)

    def chip(j):
        return lax.rem(x + j, 4)

    barrier = pltpu.get_barrier_semaphore()
    greeted = [place(1, 0), place(-1, 0), place(0, 1), place(0, -1)]
    greeted += [(ahead, tp), (behind, tp)]
    greeted += [(sp, lax.rem(tp + j, 8)) for j in range(1, 8)]
    for where in greeted:
        pl.semaphore_signal(barrier, inc=1, device_id=where, device_id_type=MESH)

    loads = [
        pltpu.make_async_copy(src, dst, local.at[i])
        for i, (src, dst) in enumerate(
            (
                (gate_hbm, gate_own), (up_hbm, up_own), (dt_hbm, dt_own), (kt_hbm, kt), (vt_hbm, vt),
                (docs_hbm, docs), (q_hbm, q), (resid_hbm, resid), (gain_hbm, gain), (op_hbm, op),
            )
        )
    ]
    for copy in loads:
        copy.start()
    for copy in loads[:3]:
        copy.wait()
    wg[z, y, :, 0:640] = gate_own[:, 0:640]
    wg[z, y, :, 768:1408] = up_own[:, 0:640]
    wg[z, y, :, 640:768] = jnp.concatenate([gate_own[:, 640:704], up_own[:, 640:704]], axis=1)
    for half in (0, 1):
        rows = slice(16 * half, 16 * half + 16)
        wd[half, 0, :, 0:640] = dt_own[rows, 0:640]
        ends = [dt_own[rows, 640:704], jnp.zeros((16, 64), BF16)]
        wd[half, 0, :, 640:768] = jnp.concatenate(ends, axis=1)
    for copy in loads[3:7]:
        copy.wait()
    pl.semaphore_wait(barrier, len(greeted))

    arrivals, leaves = {}, {}

    def index_in(table, name, amount):
        entry = table.setdefault(name, [len(table), 0])
        entry[1] += amount
        return entry[0]

    def go(name, leave, src, dst, where):
        amount = math.prod(src.shape)
        pltpu.make_async_remote_copy(
            src_ref=src, dst_ref=dst,
            send_sem=send.at[index_in(leaves, leave, amount)],
            recv_sem=recv.at[index_in(arrivals, name, amount)],
            device_id=where, device_id_type=MESH,
        ).start()

    def whole(table, name, like):
        place_of, amount = table[name]
        assert amount == math.prod(like.shape), (name, amount, like.shape)
        return pltpu.make_async_remote_copy(
            src_ref=like, dst_ref=like, send_sem=send.at[place_of], recv_sem=recv.at[place_of],
            device_id=partner, device_id_type=MESH,
        )

    def arrived(name, like):
        whole(arrivals, name, like).wait_recv()

    def left(name, like):
        whole(leaves, name, like).wait_send()

    def gu_far(half, near, far):
        dy, dz = (near, far) if half == 0 else (far, near)
        return wg.at[wrap(z, dz), wrap(y, dy), pl.ds(16 * half, 16)]

    def group_of(near):
        return next(group for group in NEARS if near in group)

    def gu_send(stage, half, sign, near):
        block = gu_far(half, near, -sign * (stage - 1))
        name = ("gu", stage, group_of(near) if stage < 4 else None)
        go(name, ("gu", stage), block, block, toward(half, 1, sign))

    def gu_first(half, sign, k):
        block = gu_far(half, -sign * (k - 1), 0)
        go(("gu first", k), "gu first", block, block, toward(half, 0, sign))

    def gu_step(k):
        arrived(("gu first", k), wg.at[0, 0 : 2 if k < 4 else 1])
        for half in (0, 1):
            for sign in BOTH:
                if k < LAST[sign]:
                    gu_first(half, sign, k + 1)
        for half in (0, 1):
            for sign in BOTH:
                if k <= LAST[sign]:
                    for way in BOTH:
                        gu_send(1, half, way, -sign * k)

    def gu_pass(stage, *nears):
        arrived(("gu", stage, nears), wg.at[0, 0 : 2 * len(nears)])
        for near in nears:
            for half in (0, 1):
                for sign in BOTH:
                    if stage < 3 or (near >= 0) == (sign > 0):
                        gu_send(stage + 1, half, sign, near)

    def dn_first(half, sign, k):
        src = wd.at[half, REL.index(-sign * (k - 1))]
        dst = wd.at[half, REL.index(-sign * k)]
        go(("dn first", k), "dn first", src, dst, toward(half, 0, sign))

    def dn_step(k):
        arrived(("dn first", k), wd.at[0, 0 : 4 if k < 4 else 2])
        for half in (0, 1):
            for sign in BOTH:
                if k < LAST[sign]:
                    dn_first(half, sign, k + 1)

    def dn_send(stage, half, sign, part):
        some = pl.ds(4 * part, 4)
        if stage == 4:
            some = pl.ds(4 * part + (0 if sign > 0 else 2), 2)
        src = wd.at[unit_of(stage - 1, half, sign), some]
        dst = wd.at[unit_of(stage, half, sign), some]
        go(("dn", stage, part), "dn", src, dst, toward(half, 1, sign))

    def dn_start(part):
        for half in (0, 1):
            for sign in BOTH:
                dn_send(1, half, sign, part)

    def dn_pass(stage, part):
        arrived(("dn", stage, part), wd.at[0:2] if stage < 4 else wd.at[0])
        if stage < 4:
            for half in (0, 1):
                for sign in BOTH:
                    dn_send(stage + 1, half, sign, part)

    for half in (0, 1):
        for sign in BOTH:
            gu_first(half, sign, 1)
    for half in (0, 1):
        for sign in BOTH:
            dn_first(half, sign, 1)
    for half in (0, 1):
        for sign in BOTH:
            gu_send(1, half, sign, 0)
    tail = pl.ds(384, 128)
    go("halo", "halo", kt.at[:, tail], hk, (ahead, tp))
    go("halo", "halo", vt.at[:, tail], hv, (ahead, tp))
    go("docs", "docs", docs, dh, (ahead, tp))

    for first, second, source in ((ka, kb, kt), (va, vb, vt)):
        first[64:128, :] = jnp.zeros((64, 640), BF16)
        second[0:64, :] = jnp.zeros((64, 640), BF16)
        first[0:64, 128:640] = source[...]
        second[64:128, 128:640] = source[...]
    for block in range(4):
        ed[0:1, 128 * (block + 1) : 128 * (block + 2)] = docs[block : block + 1, :].astype(F32)

    def attend(block):
        rows, span = pl.ds(128 * block, 128), pl.ds(128 * block, 256)
        query_docs = jnp.broadcast_to(ed[0:1, 128 * (block + 1) : 128 * (block + 2)], (128, 128)).T
        query_docs = jnp.concatenate([query_docs, query_docs], axis=1)
        at_query = lax.broadcasted_iota(jnp.int32, (128, 256), 0)
        at_key = lax.broadcasted_iota(jnp.int32, (128, 256), 1)
        visible = (at_key > at_query) & (at_key <= at_query + 128)
        visible = visible & (ed[0:1, 128 * block : 128 * block + 256] == query_docs)
        total = None
        for head, keys, vals in ((0, ka, va), (1, kb, vb)):
            scores = dot(q[rows, :], keys[:, span]) * 0.125
            scores = jnp.where(visible, scores, -jnp.inf)
            sink = sinks[head]
            top = jnp.maximum(jnp.max(scores, axis=1, keepdims=True), sink)
            raw = jnp.exp(scores - top)
            whole = jnp.sum(raw, axis=1, keepdims=True) + jnp.exp(sink - top)
            weights = (raw / whole).astype(BF16)
            part = dot_t(weights, vals[:, span])
            total = part if total is None else total + part
        att[rows, :] = total.astype(BF16)

    for block in (1, 2, 3):
        attend(block)
    gu_step(1)
    dn_step(1)
    gu_pass(1, 0)
    gu_step(2)
    gu_pass(1, -1, 1)
    dn_step(2)
    gu_pass(2, 0)
    arrived("halo", kt.at[:, 0:256])
    arrived("docs", dh)
    ka[0:64, 0:128] = hk[...]
    kb[64:128, 0:128] = hk[...]
    va[0:64, 0:128] = hv[...]
    vb[64:128, 0:128] = hv[...]
    ed[0:1, 0:128] = jnp.where(sp == 0, -1.0, dh[3:4, :].astype(F32))
    attend(0)
    lanes = pl.ds(pl.multiple_of(128 * tp, 128), 128)
    for j in range(1, 8):
        peer = lax.rem(tp + j, 8)
        rows = pl.ds(pl.multiple_of(64 * peer, 64), 64)
        go("heads", "heads", att.at[rows], at.at[:, lanes], (sp, peer))
    own_rows = pl.ds(pl.multiple_of(64 * tp, 64), 64)
    at[:, lanes] = att[own_rows, :]
    gu_step(3)
    gu_pass(1, -2, 2)
    gu_pass(2, -1, 1)
    dn_step(3)
    gu_pass(3, 0)

    arrived("heads", att.at[0:448])
    for copy in loads[7:]:
        copy.wait()
    for part in range(8):
        cols = pl.ds(256 * part, 256)
        mid[:, cols] = resid[:, cols].astype(F32) + dot(at[...], op[:, cols])
    rows64 = mid[...]
    scale = lax.rsqrt(jnp.mean(rows64 * rows64, axis=1, keepdims=True) + 1e-06)
    nb[own_rows, :] = (rows64 * scale * gain[...]).astype(BF16)
    for j in (0, 1, 3, 2):
        where = partner if j == 0 else (sp, 2 * chip(j) + core)
        go(("rows", j), "rows", nb.at[own_rows], nb.at[own_rows], where)

    def rows_on(j):
        arrived(("rows", j), nb.at[0:64])
        rows = pl.ds(pl.multiple_of(64 * (2 * chip(4 - j) + core), 64), 64)
        go(("rows", 0), "rows", nb.at[rows], nb.at[rows], partner)

    gu_step(4)
    gu_pass(1, -3, 3)
    gu_pass(2, -2, 2)
    gu_pass(3, -1, 1)
    dn_step(4)
    gu_pass(1, -4)
    gu_pass(2, -3, 3)
    gu_pass(3, -2, 2)
    rows_on(1)
    rows_on(3)
    gu_pass(2, -4)
    dn_start(0)
    gu_pass(3, -3, 3)
    rows_on(2)
    gu_pass(3, -4)
    dn_start(1)
    dn_pass(1, 0)
    arrived(("rows", 0), nb.at[0:256])
    arrived(("gu", 4, None), wg.at[0])

    def columns(first, width):
        return wg[:, :, :, first : first + width].reshape(SIDE * SIDE * 32, width)

    def silu(v):
        return v / (1.0 + jnp.exp(-v))

    def hidden_part(i):
        gate = dot(nb[...], columns(256 * i, 256))
        if i < 2:
            up = dot(nb[...], columns(768 + 256 * i, 256))
            hid[:, 256 * i : 256 * (i + 1)] = (silu(gate) * up).astype(BF16)
            return
        up = dot(nb[...], columns(1280, 128))
        hid[:, 512:640] = (silu(gate[:, :128]) * up).astype(BF16)
        mixed = gate[:, 128:]
        lane = lax.broadcasted_iota(jnp.int32, mixed.shape, 1)
        ends = silu(mixed) * pltpu.roll(mixed, 64, 1)
        hid[:, 640:768] = jnp.where(lane < 64, ends, 0.0).astype(BF16)

    def partial_of(stage):
        first = unit_of(stage, 0, 1)
        count = 2 if stage in (0, 4) else 4
        size, base = 64 * count, 128 * first
        units = wd[first : first + count].reshape(128 * count, 768)
        pb[base : base + 2 * size, :] = dot_t(units, hid[...]).astype(BF16)
        theirs = pl.ds(pl.multiple_of(base + size * other, 128), size)
        go(("pair", stage), "pair", pb.at[theirs], pr.at[pl.ds(64 * first, size)], partner)

    def chip_sum(stage):
        first = unit_of(stage, 0, 1)
        size = 128 if stage in (0, 4) else 256
        arrived(("pair", stage), pr.at[0:size])
        ours = pl.ds(pl.multiple_of(128 * first + size * core, 128), size)
        rows = pl.ds(64 * first, size)
        qb[rows, :] = (pb[ours, :].astype(F32) + pr[rows, :].astype(F32)).astype(BF16)
        for j in (2, 1, 3):
            tokens = pl.ds(pl.multiple_of(128 * chip(j), 128), 128)
            where = (sp, 2 * chip(j) + core)
            go(("sums", stage == 4), "sums", qb.at[rows, tokens], rx.at[j - 1, rows], where)

    tokens = pl.ds(pl.multiple_of(128 * x, 128), 128)

    def finish(ending):
        rows = slice(896, 1024) if ending else slice(0, 896)
        arrived(("sums", ending), rx.at[:, rows])
        mine = qb[rows, tokens].astype(F32)
        for j in range(3):
            mine = mine + rx[j, rows].astype(F32)
        ss[core, rows] = mine.astype(BF16)
        done = ss.at[core, rows]
        go(("last", ending), "last", done, done, partner)

    hidden_part(0)
    hidden_part(1)
    dn_pass(1, 1)
    hidden_part(2)
    partial_of(0)
    dn_pass(2, 0)
    partial_of(1)
    chip_sum(0)
    dn_pass(2, 1)
    chip_sum(1)
    partial_of(2)
    dn_pass(3, 0)
    chip_sum(2)
    dn_pass(3, 1)
    partial_of(3)
    chip_sum(3)
    dn_pass(4, 0)
    dn_pass(4, 1)
    partial_of(4)
    chip_sum(4)
    finish(False)
    finish(True)
    arrived(("last", False), ss.at[0, 0:896])
    arrived(("last", True), ss.at[0, 0:128])
    fars = (0, -1, 1, -2, 2, -3, 3, -4)
    for half in (0, 1):
        for i, far in enumerate(fars):
            for r, near in enumerate(REL):
                dy, dz = (near, far) if half == 0 else (far, near)
                row = 256 * wrap(z, dz) + 32 * wrap(y, dy) + 16 * half
                first = 128 * i + 16 * r
                tn[pl.ds(pl.multiple_of(row, 16), 16), :] = ss[half, first : first + 16, :].astype(F32)
    for part in range(16):
        tt[:, 128 * part : 128 * (part + 1)] = tn[128 * part : 128 * (part + 1), :].T
    out[...] = (mid[...] + tt[pl.ds(pl.multiple_of(64 * core, 64), 64), :]).astype(BF16)
    left("gu first", wg.at[0, 0:7])
    for stage in (1, 2, 3):
        left(("gu", stage), wg.at[0:2])
    left(("gu", 4), wg.at[0])
    left("dn first", wd.at[0:2, 0:7])
    left("dn", wd.at[0:14])
    left("halo", kt.at[:, 0:256])
    left("docs", dh)
    left("heads", att.at[0:448])
    left("rows", nb.at[0:448])
    left("pair", pr)
    left("sums", rx)
    left("last", ss.at[0])
    assert max(len(arrivals), len(leaves)) <= SEMS, (len(arrivals), len(leaves))


def shards(
    resid, queries, keys, values, documents, sinks, out_proj, norm_gain, gate_proj, up_proj, down_proj
):
    vmem = pl.BlockSpec(memory_space=pltpu.VMEM)
    return pl.pallas_call(
        layer,
        out_shape=jax.ShapeDtypeStruct((64, 2048), BF16),
        in_specs=[pl.BlockSpec(memory_space=pltpu.SMEM)]
        + [pl.BlockSpec(memory_space=pl.ANY)] * 10,
        out_specs=vmem,
        scratch_shapes=[
            pltpu.VMEM((64, 2048), BF16),
            pltpu.VMEM((512, 128), BF16),
            pltpu.VMEM((64, 512), BF16),
            pltpu.VMEM((64, 512), BF16),
            pltpu.VMEM((4, 128), jnp.int32),
            pltpu.VMEM((1, 2048), F32),
            pltpu.VMEM((32, 704), BF16),
            pltpu.VMEM((32, 704), BF16),
            pltpu.VMEM((32, 704), BF16),
            pltpu.VMEM((8, 8, 32, 1408), BF16),
            pltpu.VMEM((16, 8, 16, 768), BF16),
            pltpu.VMEM((1024, 2048), BF16),
            pltpu.VMEM((512, 2048), BF16),
            pltpu.VMEM((64, 1024), BF16),
            pltpu.VMEM((128, 640), BF16),
            pltpu.VMEM((128, 640), BF16),
            pltpu.VMEM((128, 640), BF16),
            pltpu.VMEM((128, 640), BF16),
            pltpu.VMEM((64, 128), BF16),
            pltpu.VMEM((64, 128), BF16),
            pltpu.VMEM((4, 128), jnp.int32),
            pltpu.VMEM((8, 640), F32),
            pltpu.VMEM((512, 128), BF16),
            pltpu.VMEM((64, 2048), F32),
            pltpu.VMEM((512, 768), BF16),
            pltpu.VMEM((2048, 512), BF16),
            pltpu.VMEM((1024, 512), BF16),
            pltpu.VMEM((1024, 512), BF16),
            pltpu.VMEM((3, 1024, 128), BF16),
            pltpu.VMEM((2, 1024, 128), BF16),
            pltpu.VMEM((2048, 128), F32),
            pltpu.VMEM((128, 2048), F32),
            pltpu.SemaphoreType.DMA((SEMS,)),
            pltpu.SemaphoreType.DMA((SEMS,)),
            pltpu.SemaphoreType.DMA((10,)),
        ],
        compiler_params=pltpu.CompilerParams(
            collective_id=0, has_side_effects=True, vmem_limit_bytes=60 * 1024 * 1024
        ),
        name="layer",
    )(
        sinks, resid, queries, keys.T, values.T, documents.reshape(4, 128),
        norm_gain.reshape(1, 2048), gate_proj, up_proj, down_proj.T, out_proj,
    )


def solution(mesh):
    in_specs = (
        P(("sp", "tp"), None),
        P("sp", "tp"),
        P("sp", "tp"),
        P("sp", "tp"),
        P("sp"),
        P("tp"),
        P(),
        P(),
        P("sp", "tp"),
        P("sp", "tp"),
        P("tp", "sp"),
    )
    out_specs = P(("sp", "tp"), None)
    return jax.shard_map(shards, mesh=mesh, in_specs=in_specs, out_specs=out_specs, check_vma=False)
```

time: 94.8 us -> 80.3 us (0.85)
  Pallas kernels: 88.3 us -> 78.5 us
  local copies, waits for them, and re-layouts: 6.09 us -> 1.67 us
    pallas_call x1, Pallas kernels: 88.3 us -> 78.5 us  [shards(): pl.pallas_call(layer, out_shape=jax.ShapeDtypeStruct((64, 2048), BF16), i...]
    concatenate x1 -> x0, local copies, waits for them, and re-layouts: 1.52 us -> none  [shards(): jnp.concatenate([gate_proj, up_proj[:, 640:], up_proj[:, :640]], axis=1)]
    slice x2 -> x0, local copies, waits for them, and re-layouts: 1.48 us -> none  [the longest x1 0.78 us: shards(): up_proj[:, :640]]
    pad x1 -> x0, local copies, waits for them, and re-layouts: 1.42 us -> none  [shards(): dn = jnp.pad(down_proj.T, ((0, 0), (0, 64)))]
where the time goes in v2:
time: 80.3 us; the launch traced here: 80.2 us
  Pallas kernels  78.5 us (98%)
  local copies, waits for them, and re-layouts  1.67 us (2%)
    pallas_call x1, Pallas kernels, shards(): pl.pallas_call(layer, out_shape=jax.ShapeDtypeStruct((64, 2048), BF16), i...  78.5 us
    unnamed x1, local copies, waits for them, and re-layouts  1.67 us

profile of v2, /device:TPU:1, one launch (start us, length us, event | category | flops | bytes accessed | tf_op | source)
XLA Modules:
  0.0 80.2 jit_solution(640678316625670734)
XLA Ops:
  0.0 78.5 %layer.1 = bf16[64,2048]{1,0:T(8,128)(2,1)} custom-call(f32[2]{0:T(128)} %sinks.1, bf16[64,2048]{1,0:T(8,128)(2,1)} %resid_hbm.1, bf16[512,128]{1,0:T(8,128)(2,1)} %q_hbm.1, bf16[64,512]{1,0:T(8,128)(2,1)} %bitcast.5, bf16[64,512]{1,0:T(8,128)(2,1)} %bitcast.6, s32[4,128]{1,0:T(4,128)} %bitcast.9, f32[1,2048]{1,0:T(1,128)} %bitcast.8, ...), custom_call_target="tpu_custom_call" | custom-call | tf_op jit(solution)/shard_map/layer/pallas_call | solution.py:410
  78.5 1.7 %copy.13 = bf16[64,2048]{1,0:T(8,128)(2,1)} copy(bf16[64,2048]{1,0:T(8,128)(2,1)} %layer.1) | data formatting | bytes 524288
